TPU v7x, 32 devices: a whole 2x2x4 slice. The times are simulated.
32 devices in a mesh: sp: 8 (over z, y), tp: 4 (over x, core).
Axes of the slice: x: 2, y: 2, z: 4, core: 2. Of those that a mesh axis runs over, the one named last changes fastest.
Arguments:
- layer_source: bfloat16 [8192, 2048], P(('sp', 'tp')), may hold values from -6 to 6
- broad_probe_tensor: bfloat16 [8192, 512], P('sp', 'tp'), may hold values from -6 to 6
- broad_retention_preact: bfloat16 [8192, 512], P('sp', 'tp'), may hold values from -6 to 6
- broad_floor_margin: float32 [512], P('tp'), may hold values from 3.6621094e-05 to 0.12
- slim_probe_tensor: bfloat16 [8192, 256], P('sp', 'tp'), may hold values from -6 to 6
- slim_retention_preact: bfloat16 [8192, 256], P('sp', 'tp'), may hold values from -6 to 6
- slim_floor_margin: float32 [256], P('tp'), may hold values from 3.6621094e-05 to 0.12
- branch_content_tensor: bfloat16 [2, 8192, 512], P(None, 'sp', 'tp'), may hold values from -6 to 6
- emitted_switch_preact: bfloat16 [2, 8192, 512], P(None, 'sp', 'tp'), may hold values from -6 to 6
- extra_log_fades: float32 [2, 8192, 4], P(None, 'sp', 'tp'), may hold values from -1.4 to 0
- channel_norm_scale: float32 [128], replicated, may hold values from 0.1 to 1.9
- emission_projection: bfloat16 [2, 512, 2048], replicated, may hold values from -0.1875 to 0.1875
- mlp_norm_scale: float32 [2048], replicated, may hold values from 0.1 to 1.9
- switch_projection: bfloat16 [2048, 5632], P('sp', 'tp'), may hold values from -0.125 to 0.125
- expand_projection: bfloat16 [2048, 5632], P('sp', 'tp'), may hold values from -0.125 to 0.125
- shrink_projection: bfloat16 [5632, 2048], P('tp', 'sp'), may hold values from -0.078125 to 0.078125
Outputs:
- layer_out: bfloat16 [8192, 2048], P(('sp', 'tp'))
All inputs are finite; a program needn't handle non-finite values.
Results may differ from a plain program's by a relative error of at most 0.0095.
Values may be sent and summed in bfloat16 or wider, within the bound.
A program may use at most 192 MiB of HBM per device.

v0:
```python
import jax
import jax.numpy as jnp
from jax import lax
from jax.sharding import PartitionSpec as P

BRANCH_CHANNELS = 4
BLOCK = 64
EPSILON = 1e-06
EXACT_PRECISION = lax.Precision.HIGHEST


def entering(part, axis, combine, identity):
    place = lax.axis_index(axis)
    gathered = jax.tree.map(lambda a: lax.all_gather(a, axis), part)
    state = jax.tree.map(lambda a, e: jnp.zeros_like(a) + jnp.asarray(e, a.dtype), part, identity)

    def one(lap, state):
        return combine(
            state, jax.tree.map(lambda a: lax.dynamic_index_in_dim(a, lap, 0, False), gathered)
        )

    return lax.fori_loop(0, place, one, state)


def switched_token_entries(
    probe_array, retention_sigmoid, floor_margin, spike_rows, rows_of_values, count_heads
):
    length = probe_array.shape[0]
    key_width = probe_array.shape[1] // count_heads
    shaped = retention_sigmoid.astype(jnp.float32).reshape(length, count_heads, key_width)
    address_entries = floor_margin.reshape(count_heads, key_width) * jax.nn.sigmoid(-shaped)
    log_fade_amount = jnp.log1p(-address_entries) + spike_rows[:, :, None]
    probe_entries = jax.nn.silu(probe_array.astype(jnp.float32)).reshape(
        length, count_heads, key_width
    ) * key_width ** (-0.5)
    content_arrays = rows_of_values.astype(jnp.float32).reshape(length, count_heads, -1)
    return (probe_entries, address_entries, log_fade_amount, content_arrays)


def block_recurrence(probe_entries, address_entries, log_fade_amount, content_arrays, block_len):
    length, count_heads, key_width = probe_entries.shape
    value_width = content_arrays.shape[2]
    block_count = length // block_len

    def to_blocks(tensor):
        return jnp.moveaxis(
            tensor.reshape(block_count, block_len, count_heads, tensor.shape[2]), 2, 1
        )

    causal_mask = jnp.tril(jnp.ones((block_len, block_len), dtype=bool))[None, :, :, None]

    def advance(carried, inputs):
        state_stack, running = carried
        block_queries, key_block, block_values, decay_block = inputs
        prefix_decay = jnp.cumsum(decay_block, axis=1)
        state_contribution = jnp.einsum(
            "yga,yau->ygu",
            block_queries * jnp.exp(prefix_decay),
            state_stack,
            precision=EXACT_PRECISION,
        )
        relative = prefix_decay[:, :, None, :] - prefix_decay[:, None, :, :]
        decays = jnp.exp(jnp.where(causal_mask, relative, -jnp.inf))
        scores = jnp.einsum(
            "htk,hsk,htsk->hts", block_queries, key_block, decays, precision=EXACT_PRECISION
        )
        inside = jnp.einsum("hts,hsv->htv", scores, block_values, precision=EXACT_PRECISION)
        total_blocks = prefix_decay[:, -1, :]
        weighted_scores = key_block * jnp.exp(total_blocks[:, None, :] - prefix_decay)
        state_stack = jnp.exp(total_blocks)[:, :, None] * state_stack + jnp.einsum(
            "xpf,xpq->xfq", weighted_scores, block_values, precision=EXACT_PRECISION
        )
        reached_state = block_queries * jnp.exp(running[:, None, :] + prefix_decay)
        return ((state_stack, running + total_blocks), (state_contribution + inside, reached_state))

    initial = (
        jnp.zeros((count_heads, key_width, value_width), jnp.float32),
        jnp.zeros((count_heads, key_width), jnp.float32),
    )
    last_carry, (output_rows, reached_state) = lax.scan(
        advance,
        initial,
        (
            to_blocks(probe_entries),
            to_blocks(address_entries),
            to_blocks(content_arrays),
            to_blocks(log_fade_amount),
        ),
    )

    def from_blocks(tensor):
        return jnp.moveaxis(tensor, 1, 2).reshape(length, count_heads, tensor.shape[3])

    return (from_blocks(output_rows), from_blocks(reached_state), last_carry)


def head_norm(output_rows, channel_norm_scale, gate_rows):
    inverse = lax.rsqrt(jnp.mean(output_rows * output_rows, axis=2, keepdims=True) + EPSILON)
    normed = (output_rows * inverse * channel_norm_scale).reshape(output_rows.shape[0], -1)
    return (normed * jax.nn.silu(gate_rows.astype(jnp.float32))).astype(jnp.bfloat16)


def combine(earlier, later):
    wide_early, wide_state_early, narrow_early, narrow_state_early = earlier
    wide_late, wide_state_late, narrow_late, narrow_state_late = later
    return (
        wide_early + wide_late,
        jnp.exp(wide_late)[:, :, None] * wide_state_early + wide_state_late,
        narrow_early + narrow_late,
        jnp.exp(narrow_late)[:, :, None] * narrow_state_early + narrow_state_late,
    )


def local(
    layer_source,
    broad_probe_tensor,
    broad_retention_preact,
    broad_floor_margin,
    slim_probe_tensor,
    slim_retention_preact,
    slim_floor_margin,
    branch_content_tensor,
    emitted_switch_preact,
    extra_log_fades,
    channel_norm_scale,
    emission_projection,
    mlp_norm_scale,
    switch_projection,
    expand_projection,
    shrink_projection,
):
    tp_count = lax.axis_size("tp")
    count_heads = BRANCH_CHANNELS // tp_count
    row_count = layer_source.shape[0]
    groups = (
        (broad_probe_tensor, broad_retention_preact, broad_floor_margin),
        (slim_probe_tensor, slim_retention_preact, slim_floor_margin),
    )
    locals_out = []
    summaries = []
    for element_ordinal in range(2):
        probe_array, retention_sigmoid, floor_margin = groups[element_ordinal]
        probe_entries, address_entries, log_fade_amount, content_arrays = switched_token_entries(
            probe_array,
            retention_sigmoid,
            floor_margin,
            extra_log_fades[element_ordinal],
            branch_content_tensor[element_ordinal],
            count_heads,
        )
        output_rows, reached_state, last_carry = block_recurrence(
            probe_entries, address_entries, log_fade_amount, content_arrays, BLOCK
        )
        locals_out.append((output_rows, reached_state))
        summaries.append(last_carry)
    wide_state, wide_log = summaries[0]
    narrow_state, narrow_log = summaries[1]
    identity = (
        jnp.zeros_like(wide_log),
        jnp.zeros_like(wide_state),
        jnp.zeros_like(narrow_log),
        jnp.zeros_like(narrow_state),
    )
    carried = entering((wide_log, wide_state, narrow_log, narrow_state), "sp", combine, identity)
    incoming_state = (carried[1], carried[3])
    mixed_parts = []
    for element_ordinal in range(2):
        output_rows, reached_state = locals_out[element_ordinal]
        output_rows = output_rows + jnp.einsum(
            "qgj,gjw->qgw",
            reached_state,
            incoming_state[element_ordinal],
            precision=EXACT_PRECISION,
        )
        mixed_parts.append(
            head_norm(output_rows, channel_norm_scale, emitted_switch_preact[element_ordinal])
        )
    mixed = jnp.concatenate(mixed_parts, axis=1)
    group_width = branch_content_tensor.shape[2]
    model_width = emission_projection.shape[2]
    regrouped = lax.all_to_all(mixed, "tp", split_axis=0, concat_axis=1, tiled=True)
    shaped = regrouped.reshape(row_count, tp_count, 2, group_width)
    branch = jnp.einsum(
        "rtgc,gtcd->rd",
        shaped,
        emission_projection.reshape(2, tp_count, group_width, model_width),
        preferred_element_type=jnp.float32,
    )
    updated = layer_source.astype(jnp.float32) + branch
    inverse = lax.rsqrt(jnp.mean(updated * updated, axis=1, keepdims=True) + EPSILON)
    normed = (updated * inverse * mlp_norm_scale).astype(jnp.bfloat16)
    gate_full, up_full, down_full = (
        lax.all_gather(switch_projection, "sp", axis=0, tiled=True),
        lax.all_gather(expand_projection, "sp", axis=0, tiled=True),
        lax.all_gather(shrink_projection, "sp", axis=1, tiled=True),
    )
    row_piece = lax.all_gather(normed, "tp", axis=0, tiled=True)
    gate_part = jnp.dot(row_piece, gate_full, preferred_element_type=jnp.float32)
    up_part = jnp.dot(row_piece, up_full, preferred_element_type=jnp.float32)
    hidden = (jax.nn.silu(gate_part) * up_part).astype(jnp.bfloat16)
    ffn_sum = lax.psum_scatter(
        jnp.dot(hidden, down_full, preferred_element_type=jnp.float32).astype(jnp.bfloat16),
        "tp",
        scatter_dimension=0,
        tiled=True,
    ).astype(jnp.float32)
    return (updated + 0.5 * ffn_sum).astype(jnp.bfloat16)


def solution(mesh):
    placed = (
        P(("sp", "tp"), None),
        P("sp", "tp"),
        P("sp", "tp"),
        P("tp"),
        P("sp", "tp"),
        P("sp", "tp"),
        P("tp"),
        P(None, "sp", "tp"),
        P(None, "sp", "tp"),
        P(None, "sp", "tp"),
        P(),
        P(),
        P(),
        P("sp", "tp"),
        P("sp", "tp"),
        P("tp", "sp"),
    )
    return jax.shard_map(
        local, mesh=mesh, in_specs=placed, out_specs=P(("sp", "tp"), None), check_vma=False
    )
```

profile of v0, /device:TPU:0, one launch (start us, length us, event | category | flops | bytes accessed | tf_op | source)
XLA Modules:
  0.0 770.1 jit_solution(4900579919354530398)
XLA Ops:
  9.6 1.8 fusion.99
  13.4 179.5 %while.51 = (s32[]{:T(128)}, f32[1,64,128]{2,1,0:T(8,128)S(1)}, f32[1,64]{1,0:T(1,128)S(1)}, f32[16,1,64,128]{3,2,1,0:T(8,128)S(1)}, f32[16,1,64,64]{3,2,1,0:T(8...) while((s32[]{:T(128)}, f32[1,64,128]{2,1,0:T(8,128)S(1)}, ...), condition=%wide.region_5.6_spmd.clone, body=%wide.region_3.5_spmd.clone.sunk | while | flops 20504708 | bytes 4946317 | solution.py:80
  15.8 1.7 select_exponential_fusion.5
  17.5 3.3 copy.114
  27.0 1.7 select_exponential_fusion.5
  28.7 3.3 copy.114
  38.2 1.7 select_exponential_fusion.5
  39.9 3.3 copy.114
  49.4 1.7 select_exponential_fusion.5
  51.1 3.3 copy.114
  60.6 1.7 select_exponential_fusion.5
  62.4 3.3 copy.114
  71.9 1.7 select_exponential_fusion.5
  73.6 3.3 copy.114
  83.1 1.7 select_exponential_fusion.5
  84.8 3.3 copy.114
  94.3 1.7 select_exponential_fusion.5
  96.0 3.3 copy.114
  105.5 1.7 select_exponential_fusion.5
  107.2 3.3 copy.114
  116.7 1.7 select_exponential_fusion.5
  118.5 3.3 copy.114
  128.0 1.7 select_exponential_fusion.5
  129.7 3.3 copy.114
  140.9 3.3 copy.114
  152.1 3.3 copy.114
  161.6 1.7 select_exponential_fusion.5
  163.4 3.3 copy.114
  174.6 3.3 copy.114
  184.1 1.7 select_exponential_fusion.5
  185.8 3.3 copy.114
  192.9 32.6 %all-gather.3 = f32[8,64,128]{2,1,0:T(8,128)S(1)} all-gather(f32[1,64,128]{2,1,0:T(8,128)S(1)} %get-tuple-element.189), channel_id=5, replica_groups=mesh['sp'=8,'tp'=4] {'sp'}, dimensions={0}, use_global_device_ids=true | all-gather | bytes 294912 | tf_op jit(solution)/shard_map/all_gather | solution.py:14
  225.5 20.6 %all-gather.5 = f32[8,1,64]{2,1,0:T(1,128)S(1)} all-gather(f32[1,1,64]{2,1,0:T(1,128)S(1)} %bitcast.343), channel_id=4, replica_groups=mesh['sp'=8,'tp'=4] {'sp'}, dimensions={0}, use_global_device_ids=true | all-gather | bytes 2304 | tf_op jit(solution)/shard_map/all_gather | solution.py:14
  248.1 2.1 divide_multiply_fusion
  250.3 64.7 %while.50 = (s32[]{:T(128)}, f32[1,128,128]{2,1,0:T(8,128)S(1)}, f32[1,128]{1,0:T(1,128)S(1)}, f32[16,1,64,128]{3,2,1,0:T(8,128)S(1)}, f32[16,1,64,128]{3,2,1,0:...) while((s32[]{:T(128)}, f32[1,128,128]{2,1,0:T(8,128)S(1)}, ...), condition=%wide.region_2.3_spmd.clone, body=%wide.region_0.2_spmd.clone.sunk | while | flops 34709760 | bytes 5176981 | solution.py:80
  315.1 31.3 %all-gather.1 = f32[8,128,128]{2,1,0:T(8,128)S(1)} all-gather(f32[1,128,128]{2,1,0:T(8,128)S(1)} %get-tuple-element.187), channel_id=3, replica_groups=mesh['sp'=8,'tp'=4] {'sp'}, dimensions={0}, use_global_device_ids=true | all-gather | bytes 589824 | tf_op jit(solution)/shard_map/all_gather | solution.py:14
  346.3 16.3 %all-gather.4 = f32[8,1,128]{2,1,0:T(1,128)S(1)} all-gather(f32[1,1,128]{2,1,0:T(1,128)S(1)} %bitcast.342), channel_id=2, replica_groups=mesh['sp'=8,'tp'=4] {'sp'}, dimensions={0}, use_global_device_ids=true | all-gather | bytes 4608 | tf_op jit(solution)/shard_map/all_gather | solution.py:14
  363.1 1.8 multiply_reduce_fusion.1
  366.6 11.4 %all_to_all.13 = bf16[4,256,256]{2,1,0:T(8,128)(2,1)S(1)} all-to-all(bf16[4,256,256]{2,1,0:T(8,128)(2,1)S(1)} %pad_maximum_fusion), channel_id=1, replica_groups=mesh['sp'=8,'tp'=4] {'tp'}, dimensions={0} | all-to-all | bytes 1048576 | tf_op jit(solution)/shard_map/all_to_all | solution.py:181
  378.2 3.9 multiply_reduce_fusion
  385.6 31.5 %all-gather.11.cloned.1.call-done = bf16[1024,2048]{1,0:T(8,128)(2,1)} async-done(((bf16[256,2048]{1,0:T(8,128)(2,1)}), bf16[1024,2048]{1,0:T(8,128)(2,1)}) %all-gather.11.cloned.1.call-update) | async-done | bytes 4194320 | tf_op jit(solution)/shard_map/all_gather | solution.py:197
  417.1 94.5 %all-gather.13.cloned.1.call-done = bf16[2048,1408]{1,0:T(8,128)(2,1)} async-done(((bf16[256,1408]{1,0:T(8,128)(2,1)}), bf16[2048,1408]{1,0:T(8,128)(2,1)}) %all-gather.13.cloned.1.call-update) | async-done | bytes 5767184 | tf_op jit(solution)/shard_map/all_gather | solution.py:193
  511.6 11.6 %fusion.101 = f32[1024,1408]{1,0:T(8,128)} fusion(bf16[1024,2048]{1,0:T(8,128)(2,1)} %all-gather.11.cloned.1.call-done, bf16[2048,1408]{1,0:T(8,128)(2,1)} %all-gather.13.cloned.1.call-done), kind=kOutput, calls=%fused_computation.155 | convolution fusion | flops 5905580032 | bytes 15728640 | tf_op jit(solution)/shard_map/dot_general | solution.py:198
  523.3 81.1 %all-gather.15.cloned.1.call-done = bf16[2048,1408]{1,0:T(8,128)(2,1)} async-done(((bf16[256,1408]{1,0:T(8,128)(2,1)}), bf16[2048,1408]{1,0:T(8,128)(2,1)}) %all-gather.15.cloned.1.call-update) | async-done | bytes 5767184 | tf_op jit(solution)/shard_map/all_gather | solution.py:194
  604.3 93.2 %all-gather.17.cloned.1.call-done = bf16[1408,2048]{1,0:T(8,128)(2,1)} async-done(((bf16[1408,256]{1,0:T(8,128)(2,1)}), bf16[1408,2048]{1,0:T(8,128)(2,1)}) %all-gather.17.cloned.1.call-update) | async-done | bytes 5767184 | tf_op jit(solution)/shard_map/all_gather | solution.py:195
  697.6 20.6 %convolution_convert_fusion = bf16[1024,2048]{1,0:T(8,128)(2,1)} fusion(bf16[1408,2048]{1,0:T(8,128)(2,1)} %all-gather.17.cloned.1.call-done, f32[1024,1408]{1,0:T(8,128)} %fusion.101, bf16[1024,2048]{1,0:T(8,128)(2,1)} %all-gather.11.cloned.1.call-done, bf16[2048,1408]{1,0:T(8,128)(2,1)} %all-gather.15.cloned.1.call-done), kind=kOutput, calls=%fused_computation.101 | convolution fusion | flops 11821907968 | bytes 25690112 | tf_op jit(solution)/shard_map/dot_general | solution.py:202
  718.2 42.9 %reduce-scatter.2.cloned.1.call-done = bf16[256,2048]{1,0:T(8,128)(2,1)} async-done(((bf16[1024,2048]{1,0:T(8,128)(2,1)}), bf16[256,2048]{1,0:T(8,128)(2,1)}) %reduce-scatter.2.cloned.1.call-update) | async-done | bytes 1048592 | tf_op jit(solution)/shard_map/reduce_scatter | solution.py:201
  761.1 2.5 add_convert_fusion
  (487 shorter events, 178.9 us)
Async XLA Ops:
  6.5 5.7 copy-start.1
  6.5 410.6 %all-gather.11.cloned.1.call-start = ((), (), s32[]{:S(2)}) async-start(), calls=%async_computation.2 | async-start | bytes 5242880 | tf_op jit(solution)/shard_map/all_gather | solution.py:197
  362.7 2.9 copy-start.3
  363.1 2.9 copy-start
  378.2 3.9 copy-start.2
  383.3 128.3 %all-gather.13.cloned.1.call-start = ((), (), s32[]{:S(2)}) async-start(), calls=%async_computation.3 | async-start | bytes 6488064 | tf_op jit(solution)/shard_map/all_gather | solution.py:193
  384.1 220.3 %all-gather.15.cloned.1.call-start = ((), (), s32[]{:S(2)}) async-start(), calls=%async_computation.4 | async-start | bytes 6488064 | tf_op jit(solution)/shard_map/all_gather | solution.py:194
  384.8 312.8 %all-gather.17.cloned.1.call-start = ((), (), s32[]{:S(2)}) async-start(), calls=%async_computation.5 | async-start | bytes 6488064 | tf_op jit(solution)/shard_map/all_gather | solution.py:195
  385.4 375.7 %reduce-scatter.2.cloned.1.call-start = ((), (), s32[]{:S(2)}) async-start(), calls=%async_computation.6 | async-start | bytes 5242880 | tf_op jit(solution)/shard_map/reduce_scatter | solution.py:201
Sparse Core Ops, SparseCore 0:
  383.4 33.6 all-gather.10
  419.3 92.3 all-gather.12
  513.8 90.4 all-gather.14
  606.2 91.2 all-gather.16
  718.3 42.7 reduce-scatter.1
where the time goes:
time: 777 us; the launch traced here: 770 us
  waiting for transfers between devices  345 us (44%)
  other arithmetic  113 us (15%)
  blocking collectives  112 us (14%)
  matrix products  97.1 us (12%)
  local copies, waits for them, and re-layouts  86.6 us (11%)
  between operations  13.4 us (2%)
    all_gather x4, blocking collectives, entering(): gathered = jax.tree.map(lambda a: lax.all_gather(a, axis), part)  101 us
    all_gather x1, waiting for transfers between devices, local(): lax.all_gather(switch_projection, 'sp', axis=0, tiled=True)  94.5 us
    all_gather x1, waiting for transfers between devices, local(): lax.all_gather(shrink_projection, 'sp', axis=1, tiled=True)  93.2 us
    all_gather x1, waiting for transfers between devices, local(): lax.all_gather(expand_projection, 'sp', axis=0, tiled=True)  81.1 us
    while x16, local copies, waits for them, and re-layouts  53.2 us
    reduce_scatter x1, waiting for transfers between devices, local(): lax.psum_scatter(jnp.dot(hidden, down_full, preferred_element_type=jnp.fl...  42.9 us
    dot_general x32, other arithmetic, advance(): jnp.einsum('htk,hsk,htsk->hts', block_queries, key_block, decays, precisi...  38.5 us
    exp x32, other arithmetic, advance(): decays = jnp.exp(jnp.where(causal_mask, relative, -jnp.inf))  37.4 us
  transfers between devices with their start and end apart: 5, of which 5 were waited for; matrix products, arithmetic and copies ran while one was open for 2% of the time, Pallas kernels for 0%

commit v1 on v0

--- a/solution.py
+++ b/solution.py
@@ -2,11 +2,16 @@
 import jax.numpy as jnp
 from jax import lax
 from jax.sharding import PartitionSpec as P
+from jax.lax import all_gather
 
 BRANCH_CHANNELS = 4
 BLOCK = 64
 EPSILON = 1e-06
 EXACT_PRECISION = lax.Precision.HIGHEST
+
+
+def _run_sectors(inner_x, lane_axis, k_dim):
+    return jnp.concatenate(all_gather(inner_x, axis_name=lane_axis), k_dim)
 
 
 def entering(part, axis, combine, identity):
@@ -192,7 +197,7 @@
     gate_full, up_full, down_full = (
         lax.all_gather(switch_projection, "sp", axis=0, tiled=True),
         lax.all_gather(expand_projection, "sp", axis=0, tiled=True),
-        lax.all_gather(shrink_projection, "sp", axis=1, tiled=True),
+        _run_sectors(shrink_projection, "sp", 1),
     )
     row_piece = lax.all_gather(normed, "tp", axis=0, tiled=True)
     gate_part = jnp.dot(row_piece, gate_full, preferred_element_type=jnp.float32)

time: 777 us -> 705 us (0.907)
  waiting for transfers between devices: 345 us -> 244 us
  local copies, waits for them, and re-layouts: 86.6 us -> 108 us
  matrix products: 97.1 us -> 106 us
    all_gather x1, waiting for transfers between devices: 93.2 us -> 0.02 us  [_run_sectors(): return jnp.concatenate(all_gather(inner_x, axis_name=lane_axis), k_dim)]
    another operation x69, local copies, waits for them, and re-layouts: 2.87 us -> 15.8 us
    dot_general x32, matrix products: 19.8 us -> 29.7 us  [advance(): jnp.einsum('hts,hsv->htv', scores, block_values, precision=EXACT_PRECISION)]
    reshape x0 -> x1, local copies, waits for them, and re-layouts: none -> 8.57 us  [_run_sectors(): return jnp.concatenate(all_gather(inner_x, axis_name=lane_axis), k_dim)]
    all_gather x1, waiting for transfers between devices: 31.5 us -> 23.4 us  [local(): row_piece = lax.all_gather(normed, 'tp', axis=0, tiled=True)]
  transfers between devices with their start and end apart: 5 -> 5, of which waited for: 5 -> 4; matrix products, arithmetic and copies ran while one was open for 2% -> 43% of each run, Pallas kernels for 0% -> 0%
where the time goes in v1:
time: 705 us; the launch traced here: 696 us
  waiting for transfers between devices  244 us (35%)
  blocking collectives  112 us (16%)
  other arithmetic  109 us (15%)
  local copies, waits for them, and re-layouts  108 us (15%)
  matrix products  106 us (15%)
  between operations  13.4 us (2%)
    all_gather x4, blocking collectives, entering(): gathered = jax.tree.map(lambda a: lax.all_gather(a, axis), part)  101 us
    all_gather x1, waiting for transfers between devices, local(): lax.all_gather(switch_projection, 'sp', axis=0, tiled=True)  94.5 us
    all_gather x1, waiting for transfers between devices, local(): lax.all_gather(expand_projection, 'sp', axis=0, tiled=True)  80.9 us
    while x16, local copies, waits for them, and re-layouts  53.2 us
    reduce_scatter x1, waiting for transfers between devices, local(): lax.psum_scatter(jnp.dot(hidden, down_full, preferred_element_type=jnp.fl...  42.9 us
    dot_general x32, other arithmetic, advance(): jnp.einsum('htk,hsk,htsk->hts', block_queries, key_block, decays, precisi...  38.8 us
    exp x32, other arithmetic, advance(): decays = jnp.exp(jnp.where(causal_mask, relative, -jnp.inf))  36.9 us
    dot_general x32, matrix products, advance(): jnp.einsum('hts,hsv->htv', scores, block_values, precision=EXACT_PRECISION)  29.7 us
  transfers between devices with their start and end apart: 5, of which 4 were waited for; matrix products, arithmetic and copies ran while one was open for 43% of the time, Pallas kernels for 0%

profile of v1, /device:TPU:0, one launch (start us, length us, event | category | flops | bytes accessed | tf_op | source)
XLA Modules:
  0.0 696.3 jit_solution(15834204758576608434)
XLA Ops:
  14.8 65.0 %while.50 = (s32[]{:T(128)}, f32[1,128,128]{2,1,0:T(8,128)S(1)}, f32[1,128]{1,0:T(1,128)S(1)}, f32[16,1,64,128]{3,2,1,0:T(8,128)S(1)}, f32[16,1,64,128]{3,2,1,0:...) while((s32[]{:T(128)}, f32[1,128,128]{2,1,0:T(8,128)S(1)}, ...), condition=%wide.region_2.3_spmd.clone, body=%wide.region_0.2_spmd.clone.sunk | while | flops 34709760 | bytes 5176981 | solution.py:85
  16.3 1.7 fusion.165
  20.4 1.7 fusion.165
  24.5 1.7 fusion.165
  28.5 1.7 fusion.165
  32.6 1.7 fusion.165
  36.6 1.7 fusion.165
  40.7 1.7 fusion.165
  44.8 1.7 fusion.165
  48.8 1.7 fusion.165
  52.9 1.7 fusion.165
  57.0 1.7 fusion.165
  61.0 1.7 fusion.165
  65.1 1.7 fusion.165
  69.2 1.7 fusion.165
  73.2 1.7 fusion.165
  77.3 1.7 fusion.165
  80.6 200.7 %while.51 = (s32[]{:T(128)}, f32[1,64,128]{2,1,0:T(8,128)S(1)}, f32[1,64]{1,0:T(1,128)S(1)}, f32[16,1,64,128]{3,2,1,0:T(8,128)}, f32[16,1,64,64]{3,2,1,0:T(8,128...) while((s32[]{:T(128)}, f32[1,64,128]{2,1,0:T(8,128)S(1)}, ...), condition=%wide.region_5.6_spmd.clone, body=%wide.region_3.5_spmd.clone.sunk | while | flops 20504708 | bytes 4913037 | solution.py:85
  84.7 3.3 copy.117
  97.2 3.3 copy.117
  109.8 3.3 copy.117
  122.3 3.3 copy.117
  134.9 3.3 copy.117
  147.4 3.3 copy.117
  160.0 3.3 copy.117
  172.5 3.3 copy.117
  185.0 3.3 copy.117
  197.6 3.3 copy.117
  210.1 3.3 copy.117
  222.7 3.3 copy.117
  235.2 3.3 copy.117
  247.8 3.3 copy.117
  260.3 3.3 copy.117
  272.9 3.3 copy.117
  282.8 22.4 %all-gather.6 = f32[8,1,64]{2,1,0:T(1,128)S(1)} all-gather(f32[1,1,64]{2,1,0:T(1,128)S(1)} %bitcast.351), channel_id=4, replica_groups=mesh['sp'=8,'tp'=4] {'sp'}, dimensions={0}, use_global_device_ids=true | all-gather | bytes 2304 | tf_op jit(solution)/shard_map/all_gather | solution.py:19
  305.2 16.3 %all-gather.5 = f32[8,1,128]{2,1,0:T(1,128)S(1)} all-gather(f32[1,1,128]{2,1,0:T(1,128)S(1)} %bitcast.352), channel_id=2, replica_groups=mesh['sp'=8,'tp'=4] {'sp'}, dimensions={0}, use_global_device_ids=true | all-gather | bytes 4608 | tf_op jit(solution)/shard_map/all_gather | solution.py:19
  321.5 31.0 %all-gather.3 = f32[8,64,128]{2,1,0:T(8,128)S(1)} all-gather(f32[1,64,128]{2,1,0:T(8,128)S(1)} %get-tuple-element.189), channel_id=5, replica_groups=mesh['sp'=8,'tp'=4] {'sp'}, dimensions={0}, use_global_device_ids=true | all-gather | bytes 294912 | tf_op jit(solution)/shard_map/all_gather | solution.py:19
  352.5 31.4 %all-gather.1 = f32[8,128,128]{2,1,0:T(8,128)S(1)} all-gather(f32[1,128,128]{2,1,0:T(8,128)S(1)} %get-tuple-element.187), channel_id=3, replica_groups=mesh['sp'=8,'tp'=4] {'sp'}, dimensions={0}, use_global_device_ids=true | all-gather | bytes 589824 | tf_op jit(solution)/shard_map/all_gather | solution.py:19
  386.4 11.4 %all_to_all.13 = bf16[4,256,256]{2,1,0:T(8,128)(2,1)S(1)} all-to-all(bf16[4,256,256]{2,1,0:T(8,128)(2,1)S(1)} %pad_maximum_fusion), channel_id=1, replica_groups=mesh['sp'=8,'tp'=4] {'tp'}, dimensions={0} | all-to-all | bytes 1048576 | tf_op jit(solution)/shard_map/all_to_all | solution.py:186
  398.0 3.9 multiply_reduce_fusion
  404.7 8.6 %copy.87 = bf16[1408,8,256]{0,2,1:T(8,128)(2,1)} copy(bf16[1408,8,256]{2,0,1:T(8,128)(2,1)} %bitcast.329) | data formatting | bytes 11534336 | tf_op jit(solution)/shard_map/reshape | solution.py:14
  413.2 23.4 %all-gather.12.cloned.1.call-done = bf16[1024,2048]{1,0:T(8,128)(2,1)} async-done(((bf16[256,2048]{1,0:T(8,128)(2,1)}), bf16[1024,2048]{1,0:T(8,128)(2,1)}) %all-gather.12.cloned.1.call-update) | async-done | bytes 4194320 | tf_op jit(solution)/shard_map/all_gather | solution.py:202
  436.7 94.5 %all-gather.14.cloned.1.call-done = bf16[2048,1408]{1,0:T(8,128)(2,1)} async-done(((bf16[256,1408]{1,0:T(8,128)(2,1)}), bf16[2048,1408]{1,0:T(8,128)(2,1)}) %all-gather.14.cloned.1.call-update) | async-done | bytes 5767184 | tf_op jit(solution)/shard_map/all_gather | solution.py:198
  531.2 11.7 %fusion.101 = f32[1024,1408]{1,0:T(8,128)} fusion(bf16[1024,2048]{1,0:T(8,128)(2,1)} %all-gather.12.cloned.1.call-done, bf16[2048,1408]{1,0:T(8,128)(2,1)} %all-gather.14.cloned.1.call-done), kind=kOutput, calls=%fused_computation.155 | convolution fusion | flops 5905580032 | bytes 15728640 | tf_op jit(solution)/shard_map/dot_general | solution.py:203
  542.9 80.9 %all-gather.16.cloned.1.call-done = bf16[2048,1408]{1,0:T(8,128)(2,1)} async-done(((bf16[256,1408]{1,0:T(8,128)(2,1)}), bf16[2048,1408]{1,0:T(8,128)(2,1)}) %all-gather.16.cloned.1.call-update) | async-done | bytes 5767184 | tf_op jit(solution)/shard_map/all_gather | solution.py:199
  623.7 20.6 %convolution_convert_fusion = bf16[1024,2048]{1,0:T(8,128)(2,1)} fusion(bf16[1408,2048]{0,1:T(8,128)(2,1)} %bitcast.330, f32[1024,1408]{1,0:T(8,128)} %fusion.101, bf16[1024,2048]{1,0:T(8,128)(2,1)} %all-gather.12.cloned.1.call-done, bf16[2048,1408]{1,0:T(8,128)(2,1)} %all-gather.16.cloned.1.call-done), kind=kOutput, calls=%fused_computation.101 | convolution fusion | flops 11821907968 | bytes 25690112 | tf_op jit(solution)/shard_map/dot_general | solution.py:207
  644.4 42.9 %reduce-scatter.2.cloned.1.call-done = bf16[256,2048]{1,0:T(8,128)(2,1)} async-done(((bf16[1024,2048]{1,0:T(8,128)(2,1)}), bf16[256,2048]{1,0:T(8,128)(2,1)}) %reduce-scatter.2.cloned.1.call-update) | async-done | bytes 1048592 | tf_op jit(solution)/shard_map/reduce_scatter | solution.py:206
  687.3 2.5 add_convert_fusion
  (498 shorter events, 198.4 us)
Async XLA Ops:
  6.5 4.8 copy-start.1
  6.5 5.7 copy-start.5
  6.5 398.1 %all-gather.18.cloned.1.call-start = ((), (), s32[]{:S(2)}) async-start(), calls=%async_computation.6 | async-start | bytes 6488064 | tf_op jit(solution)/shard_map/all_gather | solution.py:14
  7.3 429.4 %all-gather.12.cloned.1.call-start = ((), (), s32[]{:S(2)}) async-start(), calls=%async_computation.2 | async-start | bytes 5242880 | tf_op jit(solution)/shard_map/all_gather | solution.py:202
  8.1 5.3 copy-start.3
  10.3 3.3 copy-start.4
  10.3 3.3 copy-start.7
  282.8 101.1 %copy-start = (f32[16,1,64,64]{3,2,1,0:T(8,128)S(1)}, f32[16,1,64,64]{3,2,1,0:T(8,128)}, u32[]{:S(2)}) copy-start(f32[16,1,64,64]{3,2,1,0:T(8,128)} %get-tuple-element.194) | copy-start | bytes 786436
  352.5 32.8 %copy-start.8 = (f32[128]{0:T(128)S(1)}, f32[128]{0:T(128)}, u32[]{:S(2)}) copy-start(f32[128]{0:T(128)} %param.32) | copy-start | bytes 1540
  384.6 1.3 copy-start.2
  398.0 3.9 copy-start.6
  403.1 128.1 %all-gather.14.cloned.1.call-start = ((), (), s32[]{:S(2)}) async-start(), calls=%async_computation.3 | async-start | bytes 6488064 | tf_op jit(solution)/shard_map/all_gather | solution.py:198
  403.8 219.9 %all-gather.16.cloned.1.call-start = ((), (), s32[]{:S(2)}) async-start(), calls=%async_computation.4 | async-start | bytes 6488064 | tf_op jit(solution)/shard_map/all_gather | solution.py:199
  404.4 282.9 %reduce-scatter.2.cloned.1.call-start = ((), (), s32[]{:S(2)}) async-start(), calls=%async_computation.5 | async-start | bytes 5242880 | tf_op jit(solution)/shard_map/reduce_scatter | solution.py:206
Sparse Core Ops, SparseCore 0:
  9.5 95.2 all-gather.17
  403.2 33.4 all-gather.11
  438.8 92.3 all-gather.13
  533.2 90.4 all-gather.15
  644.5 42.7 reduce-scatter.1
